TPU v7x, 32 devices: a whole 2x2x4 slice. The times are simulated.
32 devices in a mesh: sp: 8 (over z, y), tp: 4 (over x, core).
Axes of the slice: x: 2, y: 2, z: 4, core: 2. Of those that a mesh axis runs over, the one named last changes fastest.
Arguments:
- tokens: bfloat16 [1024, 2048], P('sp', 'tp'), may hold values from -28 to 28
- norm_gain: bfloat16 [1, 2048], P(None, 'tp'), may hold values from 0.099609375 to 1.8984375
- conv_b_w: bfloat16 [2048, 1024], P(None, 'tp'), may hold values from -0.125 to 0.125
- conv_c_w: bfloat16 [2048, 1024], P(None, 'tp'), may hold values from -0.125 to 0.125
- conv_u_w: bfloat16 [2048, 1024], P(None, 'tp'), may hold values from -0.125 to 0.125
- conv_taps: bfloat16 [3, 1024], P(None, 'tp'), may hold values from -3.5 to 3.5
- query_w: bfloat16 [2048, 2048], P(None, 'tp'), may hold values from -0.125 to 0.125
- key_w: bfloat16 [2048, 2048], P(None, 'tp'), may hold values from -0.125 to 0.125
- value_w: bfloat16 [2048, 2048], P(None, 'tp'), may hold values from -0.125 to 0.125
- outgate_w: bfloat16 [2048, 2048], P(None, 'tp'), may hold values from -0.125 to 0.125
- gate_w: bfloat16 [2048, 2, 8], P(None, None, 'tp'), may hold values from -0.125 to 0.125
- gate_bias: float32 [2, 8], P(None, 'tp'), may hold values from -5 to 150
- mem_gain: bfloat16 [2048], P('tp'), may hold values from 0.099609375 to 1.8984375
- conv_out_w: bfloat16 [1024, 2048], P('tp'), may hold values from -0.1875 to 0.1875
- mem_out_w: bfloat16 [2048, 2048], P('tp'), may hold values from -0.125 to 0.125
Outputs:
- layer_out: bfloat16 [1024, 2048], P(('sp', 'tp'))
All inputs are finite; a program needn't handle non-finite values.
Results may differ from a plain program's by a relative error of at most 0.014.
The roundings to bfloat16 on the way count: a program that leaves them out, or rounds other values in their place, can miss the bound.
Values may be sent and summed in bfloat16 or wider, within the bound.
A program may use at most 64 MiB of HBM per device.

v0:
```python
import jax
import jax.numpy as jnp
from jax import lax
from jax.sharding import PartitionSpec as P

HEAD_DIM = 256
BLOCK = 128
MDIM = 2048
EPS = 1e-06
LOWEST = -1e30
HIGH = lax.Precision.HIGHEST


def shifted(value, axis, by):
    count = lax.axis_size(axis)
    pairs = [(i, i + by) for i in range(count) if 0 <= i + by < count]
    return lax.ppermute(value, axis, pairs)


def prefix(value, axis, join, neutral):
    count, mine = (lax.axis_size(axis), lax.axis_index(axis))
    pieces = jax.tree.map(lambda part: lax.all_gather(part, axis), value)
    total = jax.tree.map(
        lambda part, zero: jnp.full_like(part, 0) + jnp.asarray(zero, part.dtype), value, neutral
    )

    def prefix_step(position, total):
        longer = join(total, jax.tree.map(lambda part: part[position], pieces))
        return jax.tree.map(lambda new, old: jnp.where(position < mine, new, old), longer, total)

    return lax.fori_loop(0, count - 1, prefix_step, total)


def local_pass(queries, keys, values, input_pre, log_forget):
    count, width = queries.shape
    blocks = count // BLOCK

    def local_step(carry, inputs):
        memory, normer, stabil, decay_sum = carry
        query_block, key_block, value_block, input_gate, forget_block = inputs
        causal = jnp.tril(jnp.ones((BLOCK, BLOCK), dtype=bool))
        running = jnp.cumsum(forget_block)
        decays = jnp.where(
            causal, running[:, None] - running[None, :] + input_gate[None, :], -jnp.inf
        )
        inter = running + stabil
        row_max = jnp.maximum(inter, jnp.max(decays, axis=1))
        weights = jnp.exp(decays - row_max[:, None])
        scores = jnp.dot(query_block, key_block.T, precision=HIGH) * weights
        carried = jnp.exp(inter - row_max)
        numer_part = carried[:, None] * jnp.dot(query_block, memory, precision=HIGH) + jnp.dot(
            scores, value_block, precision=HIGH
        )
        denom_part = carried * jnp.dot(query_block, normer, precision=HIGH) + jnp.sum(
            scores, axis=1
        )
        new_stabil = row_max[-1]
        key_weight = jnp.exp(running[-1] - running + input_gate - new_stabil)
        fade = jnp.exp(running[-1] + stabil - new_stabil)
        memory = fade * memory + jnp.dot(
            (key_weight[:, None] * key_block).T, value_block, precision=HIGH
        )
        normer = fade * normer + jnp.dot(key_weight, key_block, precision=HIGH)
        outputs = (numer_part, denom_part, row_max, decay_sum + running)
        return ((memory, normer, new_stabil, decay_sum + running[-1]), outputs)

    inputs = (
        queries.reshape(blocks, BLOCK, width),
        keys.reshape(blocks, BLOCK, width),
        values.reshape(blocks, BLOCK, width),
        input_pre.reshape(blocks, BLOCK),
        log_forget.reshape(blocks, BLOCK),
    )
    start = (
        jnp.zeros((width, width), jnp.float32),
        jnp.zeros((width,), jnp.float32),
        jnp.zeros((), jnp.float32),
        jnp.zeros((), jnp.float32),
    )
    final, rows = lax.scan(local_step, start, inputs)
    memory, normer, stabil, decay_sum = final
    numer_rows, denom_rows, row_max, row_decay = rows
    return (
        numer_rows.reshape(count, width),
        denom_rows.reshape(count),
        row_max.reshape(count),
        row_decay.reshape(count),
        decay_sum,
        stabil,
        memory,
        normer,
    )


def finish(queries, numer_rows, denom_rows, row_max, row_decay, stabil_in, memory_in, normer_in):
    from_before = jnp.dot(queries, memory_in, precision=HIGH)
    normer_before = jnp.dot(queries, normer_in, precision=HIGH)
    top = jnp.maximum(row_max, row_decay + stabil_in)
    own_scale = jnp.exp(row_max - top)
    past_scale = jnp.exp(row_decay + stabil_in - top)
    numer_all = own_scale[:, None] * numer_rows + past_scale[:, None] * from_before
    denom_all = own_scale * denom_rows + past_scale * normer_before
    return numer_all / jnp.maximum(jnp.abs(denom_all), jnp.exp(-top))[:, None]


def join_state(earlier, later):
    sum_early, stab_early, mem_early, norm_early = earlier[:4]
    sum_late, stab_late, mem_late, norm_late = later[:4]
    top = jnp.maximum(sum_late + stab_early, stab_late)
    early_scale = jnp.exp(sum_late + stab_early - top)
    late_scale = jnp.exp(stab_late - top)
    joined = (
        sum_early + sum_late,
        top,
        early_scale[:, None, None] * mem_early + late_scale[:, None, None] * mem_late,
        early_scale[:, None] * norm_early + late_scale[:, None] * norm_late,
    )
    if len(earlier) > 4:
        edge = jnp.where(later[5][0] > 0, later[4], earlier[4])
        joined = joined + (edge, jnp.maximum(earlier[5], later[5]))
    return joined


def body(
    tokens,
    norm_gain,
    conv_b_w,
    conv_c_w,
    conv_u_w,
    conv_taps,
    query_w,
    key_w,
    value_w,
    outgate_w,
    gate_w,
    gate_bias,
    mem_gain,
    conv_out_w,
    mem_out_w,
):
    count = tokens.shape[0]
    model = conv_b_w.shape[0]
    weights = (
        conv_b_w,
        conv_c_w,
        conv_u_w,
        query_w,
        key_w,
        value_w,
        outgate_w,
        gate_w.reshape(model, -1),
    )
    piece = lax.all_gather(tokens, "tp", axis=1, tiled=True)
    gain_piece = lax.all_gather(norm_gain, "tp", axis=1, tiled=True)
    wide = piece.astype(jnp.float32)
    scaled = (wide * gain_piece.astype(jnp.float32)).astype(jnp.bfloat16)
    squares = jnp.sum(wide * wide, axis=1)
    totals = tuple(
        (jnp.dot(scaled, weight, preferred_element_type=jnp.float32) for weight in weights)
    )
    folded = (squares,) + totals
    inv_rms = lax.rsqrt(folded[0] / model + EPS)[:, None]

    def project(total):
        return lax.optimization_barrier((inv_rms * total).astype(jnp.bfloat16)).astype(jnp.float32)

    gate_b, gate_c, gate_u, queries, keys, values, outgate = [
        project(total) for total in folded[1:8]
    ]
    heads = gate_bias.shape[1]
    gates = inv_rms * folded[8]
    input_pre = gates[:, :heads] + gate_bias[0]
    forget_pre = gates[:, heads:] + gate_bias[1]
    mixed_in = (gate_c * gate_u).astype(jnp.bfloat16)
    reach = conv_taps.shape[0] - 1
    head_q = queries.reshape(count, heads, HEAD_DIM)
    head_k = keys.reshape(count, heads, HEAD_DIM) * HEAD_DIM ** (-0.5)
    head_v = values.reshape(count, heads, HEAD_DIM)
    local = jax.vmap(local_pass, in_axes=1, out_axes=(1, 1, 1, 1, 0, 0, 0, 0))(
        head_q, head_k, head_v, input_pre, jax.nn.log_sigmoid(forget_pre)
    )
    numer_rows, denom_rows, row_max, row_decay, decay_sum, stabil, memory, normer = local
    identity = (
        jnp.zeros((heads,), jnp.float32),
        jnp.full((heads,), LOWEST, jnp.float32),
        jnp.zeros((heads, HEAD_DIM, HEAD_DIM), jnp.float32),
        jnp.zeros((heads, HEAD_DIM), jnp.float32),
    )
    before = shifted(mixed_in[count - reach :], "sp", 1)
    incoming = prefix((decay_sum, stabil, memory, normer), "sp", join_state, identity)
    padded = jnp.concatenate([before, mixed_in], axis=0).astype(jnp.float32)
    taps = conv_taps.astype(jnp.float32)
    conv_sum = taps[0] * padded[0:count]
    for offset in range(1, reach + 1):
        conv_sum = conv_sum + taps[offset] * padded[offset : offset + count]
    y_conv = (gate_b * conv_sum).astype(jnp.bfloat16)
    mem_raw = jax.vmap(finish, in_axes=(1, 1, 1, 1, 1, 0, 0, 0), out_axes=1)(
        head_q, numer_rows, denom_rows, row_max, row_decay, incoming[1], incoming[2], incoming[3]
    )
    flat_raw = mem_raw.reshape(count, -1)
    own_squares = jnp.sum(flat_raw * flat_raw, axis=1)
    all_squares = lax.psum(own_squares, "tp")
    mem_norm = flat_raw * lax.rsqrt(all_squares / MDIM + EPS)[:, None]
    mem_norm = mem_norm * mem_gain.astype(jnp.float32)[None, :]
    y_mem = (jax.nn.sigmoid(outgate) * mem_norm).astype(jnp.bfloat16)
    return lax.psum_scatter(
        (
            jnp.dot(y_conv, conv_out_w, preferred_element_type=jnp.float32)
            + jnp.dot(y_mem, mem_out_w, preferred_element_type=jnp.float32)
        ).astype(jnp.bfloat16),
        "tp",
        scatter_dimension=0,
        tiled=True,
    )


def solution(mesh):
    return jax.shard_map(
        body,
        mesh=mesh,
        in_specs=(
            P("sp", "tp"),
            P(None, "tp"),
            P(None, "tp"),
            P(None, "tp"),
            P(None, "tp"),
            P(None, "tp"),
            P(None, "tp"),
            P(None, "tp"),
            P(None, "tp"),
            P(None, "tp"),
            P(None, None, "tp"),
            P(None, "tp"),
            P("tp"),
            P("tp", None),
            P("tp", None),
        ),
        out_specs=P(("sp", "tp"), None),
        check_vma=False,
    )
```

profile of v0, /device:TPU:0, one launch (start us, length us, event | category | flops | bytes accessed | tf_op | source)
XLA Modules:
  0.0 148.9 jit_solution(2480114630991469454)
XLA Ops:
  6.6 0.8 slice_bitcast_fusion
  7.4 6.3 %all_gather.31 = bf16[1,2048]{1,0:T(2,128)(2,1)S(1)} all-gather(bf16[1,512]{1,0:T(2,128)(2,1)} %param.18), channel_id=1, replica_groups=mesh['sp'=8,'tp'=4] {'tp'}, dimensions={1}, use_global_device_ids=true | all-gather | bytes 5120 | tf_op jit(solution)/shard_map/all_gather | solution.py:154
  13.7 0.7 reshape.140
  14.5 7.9 %all_gather.30 = bf16[128,2048]{1,0:T(8,128)(2,1)S(1)} all-gather(bf16[128,512]{1,0:T(8,128)(2,1)} %param.17), channel_id=1, replica_groups=mesh['sp'=8,'tp'=4] {'tp'}, dimensions={1}, use_global_device_ids=true | all-gather | bytes 655360 | tf_op jit(solution)/shard_map/all_gather | solution.py:153
  22.3 0.2 fusion.21
  22.5 0.2 convolution_multiply_fusion.8
  22.8 0.1 add_bitcast_fusion
  22.9 0.3 reduce_window_sum.14
  23.2 0.1 fusion.41
  23.3 0.2 multiply_reduce_fusion.1
  23.6 0.1 subtract_exponential_fusion.4
  23.7 2.2 %fusion.15 = bf16[128,512]{1,0:T(8,128)(2,1)S(1)} fusion(bf16[2048,512]{1,0:T(8,128)(2,1)} %param.24, f32[128]{0:T(128)S(1)} %add_rsqrt_fusion.1, bf16[128,2048]{1,0:T(8,128)(2,1)S(1)} %all_gather.30, f32[2048]{0:T(1024)S(1)} %bitcast.213), kind=kOutput, calls=%fused_computation.34 | convolution fusion | flops 269352960 | bytes 2761216 | tf_op jit(solution)/shard_map/dot_general | solution.py:159
  25.9 0.4 fusion.16
  26.4 1.3 convolution_add_fusion.1
  27.7 0.0 all-gather.7.cloned.1.call-update
  27.7 0.0 reduce-scatter.2.cloned.1.call-start
  27.7 1.5 %fusion.19 = bf16[128,256]{1,0:T(8,128)(2,1)S(1)} fusion(bf16[2048,256]{1,0:T(8,128)(2,1)} %param.20, f32[128]{0:T(128)S(1)} %add_rsqrt_fusion.1, bf16[128,2048]{1,0:T(8,128)(2,1)S(1)} %all_gather.30, f32[2048]{0:T(1024)S(1)} %bitcast.215), kind=kOutput, calls=%fused_computation.42 | convolution fusion | flops 135069696 | bytes 1647104 | tf_op jit(solution)/shard_map/dot_general | solution.py:159
  29.3 0.0 copy-start.4
  29.3 1.5 %fusion.20 = bf16[128,256]{1,0:T(8,128)(2,1)S(1)} fusion(bf16[2048,256]{1,0:T(8,128)(2,1)} %param.21, f32[128]{0:T(128)S(1)} %add_rsqrt_fusion.1, bf16[128,2048]{1,0:T(8,128)(2,1)S(1)} %all_gather.30, f32[2048]{0:T(1024)S(1)} %bitcast.216), kind=kOutput, calls=%fused_computation.43 | convolution fusion | flops 135069696 | bytes 1647104 | tf_op jit(solution)/shard_map/dot_general | solution.py:159
  30.9 3.5 %collective-permute-start = (bf16[2,256]{1,0:T(2,128)(2,1)S(1)}, bf16[2,256]{1,0:T(2,128)(2,1)S(1)}, u32[]{:S(2)}, u32[]{:S(2)}) collective-permute-start(bf16[2,256]{1,0:T(2,128)(2,1)S(1)} %slice.57), channel_id=1, source_target_pairs={{0,4},{4,8},{8,12},{12,16},{16,20},{20,24},{24,28},{1,5},{5,9},{9,... | collective-permute-start | bytes 3080 | tf_op jit(solution)/shard_map/ppermute | solution.py:17
  34.4 0.6 dynamic-slice.10
  35.7 0.2 dynamic-update-slice
  35.9 0.2 dynamic-update-slice.1
  36.1 2.3 %fusion.17 = bf16[128,512]{1,0:T(8,128)(2,1)S(1)} fusion(bf16[2048,512]{1,0:T(8,128)(2,1)} %param.23, f32[128]{0:T(128)S(1)} %add_rsqrt_fusion.1, bf16[128,2048]{1,0:T(8,128)(2,1)S(1)} %all_gather.30, f32[2048]{0:T(1024)S(1)} %bitcast.217), kind=kOutput, calls=%fused_computation.36 | convolution fusion | flops 269352960 | bytes 2761216 | tf_op jit(solution)/shard_map/dot_general | solution.py:159
  38.4 0.0 copy-start.2
  38.4 0.2 fusion.23
  38.7 0.1 fusion.63
  38.8 0.2 fusion.33
  38.9 0.3 fusion.80
  39.3 0.3 convolution_bitcast_fusion.2
  39.6 0.0 copy-start.5
  39.6 0.3 fusion.18
  39.9 0.1 copy-done.2
  40.0 0.4 fusion.14
  40.5 27.0 %all-gather.4 = f32[8,2,256]{2,1,0:T(2,128)S(1)} all-gather(f32[1,2,256]{2,1,0:T(2,128)S(1)} %fusion.63), channel_id=5, replica_groups=mesh['sp'=8,'tp'=4] {'sp'}, dimensions={0}, use_global_device_ids=true | all-gather | bytes 18432 | tf_op jit(solution)/shard_map/all_gather | solution.py:22
  67.5 19.8 %all-reduce.2 = (f32[16]{0:T(128)S(1)}, f32[16]{0:T(128)S(1)}) all-reduce(f32[16]{0:T(128)S(1)} %dynamic-update-slice, f32[16]{0:T(128)S(1)} %dynamic-update-slice.1), channel_id=2, replica_groups=mesh['sp'=8,'tp'=4] {'sp'}, use_global_device_ids=true, to_apply=%add | all-reduce | flops 32 | bytes 256
  87.3 0.1 reshape.145
  87.4 0.1 reshape.146
  87.5 0.0 collective-permute-done
  87.5 2.5 %fusion.50 = f32[128,2048]{1,0:T(8,128)} fusion(bf16[256,2048]{1,0:T(8,128)(2,1)} %param.30, f32[130,256]{1,0:T(8,128)S(1)} %maximum_convert_fusion, bf16[128,256]{1,0:T(8,128)(2,1)S(1)} %fusion.18, f32[256]{0:T(256)S(1)} %bitcast.230, f32[256]{0:T(256)S(1)} %bitcast.229, f32[256]{0:T(256)S(1)} %bitcast.228), kind=kOutput, calls=%fused_computation.85 | convolution fusion | flops 134479872 | bytes 2558976 | tf_op jit(solution)/shard_map/dot_general | solution.py:208
  90.1 12.7 %all-gather.7.cloned.1.call-done = f32[16,256,256]{2,1,0:T(8,128)} async-done(((f32[2,256,256]{2,1,0:T(8,128)}), f32[16,256,256]{2,1,0:T(8,128)}) %all-gather.7.cloned.1.call-update) | async-done | bytes 4194320 | tf_op jit(solution)/shard_map/all_gather | solution.py:22
  102.8 9.3 %while.5 = (s32[]{:T(128)}, f32[2]{0:T(128)S(1)}, f32[2,256,256]{2,1,0:T(8,128)S(1)}, f32[2,256]{1,0:T(2,128)S(1)}, s32[]{:T(128)}, /*index=5*/f32[8,2]{1,0:T(8,...) while((s32[]{:T(128)}, f32[2]{0:T(128)S(1)}, ...), condition=%wide.region_4.5_spmd.clone, body=%wide.region_3.4_spmd.clone.sunk | while | flops 657940 | bytes 1579278 | solution.py:31
  102.8 0.1 fusion.97
  102.9 1.2 fusion.96
  104.2 0.1 fusion.97
  104.3 1.2 fusion.96
  105.5 0.1 fusion.97
  105.6 1.2 fusion.96
  106.9 0.1 fusion.97
  106.9 1.2 fusion.96
  108.2 0.1 fusion.97
  108.3 1.2 fusion.96
  109.5 0.1 fusion.97
  109.6 1.2 fusion.96
  110.9 0.1 fusion.97
  111.0 1.2 fusion.96
  112.1 0.2 fusion.31
  112.3 0.1 fusion.71
  112.4 0.3 fusion.13
  112.7 0.5 multiply_reduce_fusion
  113.2 5.7 %psum.7 = f32[128]{0:T(128)S(1)} all-reduce(f32[128]{0:T(128)S(1)} %get-tuple-element.276), channel_id=1, replica_groups=mesh['sp'=8,'tp'=4] {'tp'}, use_global_device_ids=true, to_apply=%region_7.8 | all-reduce | flops 128 | bytes 1024 | tf_op jit(solution)/shard_map/psum | solution.py:202
  118.9 2.5 %fusion.7 = bf16[128,2048]{1,0:T(8,128)(2,1)} fusion(f32[128,2048]{1,0:T(8,128)} %fusion.50, bf16[512,2048]{1,0:T(8,128)(2,1)S(1)} %copy-done, f32[128,512]{1,0:T(8,128)S(1)} %bitcast.211, bf16[128,512]{1,0:T(8,128)(2,1)S(1)} %fusion.14, f32[512]{0:T(512)S(1)} %convert_element_type.84, f32[128]{0:T(128)S(1)} %add_rsqrt_fusion), kind=kOutput, calls=%fused_computation.16 | convolution fusion | flops 269484032 | bytes 4065792 | tf_op jit(solution)/shard_map/dot_general | solution.py:209
  121.4 0.0 reduce-scatter.2.cloned.1.call-update
  121.4 20.7 %reduce-scatter.2.cloned.1.call-done = bf16[32,2048]{1,0:T(8,128)(2,1)} async-done(((bf16[128,2048]{1,0:T(8,128)(2,1)}), bf16[32,2048]{1,0:T(8,128)(2,1)}) %reduce-scatter.2.cloned.1.call-update) | async-done | bytes 131088 | tf_op jit(solution)/shard_map/reduce_scatter | solution.py:206
  (43 shorter events, 0.4 us)
Async XLA Ops:
  6.5 112.4 %copy-start = (bf16[512,2048]{1,0:T(8,128)(2,1)S(1)}, bf16[512,2048]{1,0:T(8,128)(2,1)}, u32[]{:S(2)}) copy-start(bf16[512,2048]{1,0:T(8,128)(2,1)} %param.31) | copy-start | bytes 6291460
  6.5 96.3 %all-gather.7.cloned.1.call-start = ((), (), s32[]{:S(2)}) async-start(), calls=%async_computation.2 | async-start | bytes 4718592 | tf_op jit(solution)/shard_map/all_gather | solution.py:22
  23.2 2.7 %copy-start.1 = (bf16[2048,512]{1,0:T(8,128)(2,1)S(1)}, bf16[2048,512]{1,0:T(8,128)(2,1)}, u32[]{:S(2)}) copy-start(bf16[2048,512]{1,0:T(8,128)(2,1)} %param.25) | copy-start | bytes 6291460
  27.7 6.8 %copy-start.6 = (u32[32]{0:T(128)S(1)}, u32[32]{0:T(128)}, u32[]{:S(2)}) copy-start(u32[32]{0:T(128)} %constant.86) | copy-start | bytes 388
  27.7 114.4 %reduce-scatter.2.cloned.1.call-start = ((), (), s32[]{:S(2)}) async-start(), calls=%async_computation.1 | async-start | bytes 655360 | tf_op jit(solution)/shard_map/reduce_scatter | solution.py:206
  29.3 9.5 %copy-start.4 = (bf16[3,256]{1,0:T(4,128)(2,1)S(1)}, bf16[3,256]{1,0:T(4,128)(2,1)}, u32[]{:S(2)}) copy-start(bf16[3,256]{1,0:T(4,128)(2,1)} %param.22) | copy-start | bytes 4612
  30.9 56.6 %collective-permute-start = (bf16[2,256]{1,0:T(2,128)(2,1)S(1)}, bf16[2,256]{1,0:T(2,128)(2,1)S(1)}, u32[]{:S(2)}, u32[]{:S(2)}) collective-permute-start(bf16[2,256]{1,0:T(2,128)(2,1)S(1)} %slice.57), channel_id=1, source_target_pairs={{0,4},{4,8},{8,12},{12,16},{16,20},{20,24},{24,28},{1,5},{5,9},{9,... | collective-permute-start | bytes 3080 | tf_op jit(solution)/shard_map/ppermute | solution.py:17
  36.1 3.5 %copy-start.3 = (bf16[2048,256]{1,0:T(8,128)(2,1)S(1)}, bf16[2048,256]{1,0:T(8,128)(2,1)}, u32[]{:S(2)}) copy-start(bf16[2048,256]{1,0:T(8,128)(2,1)} %param.19) | copy-start | bytes 3145732
  38.4 1.6 %copy-start.2 = (bf16[2048,512]{1,0:T(8,128)(2,1)S(1)}, bf16[2048,512]{1,0:T(8,128)(2,1)}, u32[]{:S(2)}) copy-start(bf16[2048,512]{1,0:T(8,128)(2,1)} %param.26) | copy-start | bytes 6291460
  39.6 47.7 %copy-start.5 = (bf16[512]{0:T(512)(128)(2,1)S(1)}, bf16[512]{0:T(512)(128)(2,1)}, u32[]{:S(2)}) copy-start(bf16[512]{0:T(512)(128)(2,1)} %param.29) | copy-start | bytes 3076
Sparse Core Ops, SparseCore 0:
  27.8 74.9 all-gather.6
  121.6 20.4 reduce-scatter.1
where the time goes:
time: 150 us; the launch traced here: 149 us
  blocking collectives  66.7 us (44%)
  waiting for transfers between devices  33.4 us (22%)
  matrix products  17.4 us (12%)
  between operations  14.3 us (10%)
  other arithmetic  10.4 us (7%)
  starting transfers between devices  3.57 us (2%)
  local copies, waits for them, and re-layouts  2.92 us (2%)
    all_gather x1, blocking collectives, prefix(): pieces = jax.tree.map(lambda part: lax.all_gather(part, axis), value)  27 us
    reduce_scatter x1, waiting for transfers between devices, body(): lax.psum_scatter((jnp.dot(y_conv, conv_out_w, preferred_element_type=jnp....  20.7 us
    unnamed x1, blocking collectives  19.8 us
    all_gather x1, waiting for transfers between devices, prefix(): pieces = jax.tree.map(lambda part: lax.all_gather(part, axis), value)  12.7 us
    dot_general x8, matrix products, body(): jnp.dot(scaled, weight, preferred_element_type=jnp.float32)  9 us
    select_n x14, other arithmetic, prefix_step(): jnp.where(position < mine, new, old)  8.88 us
    all_gather x1, blocking collectives, body(): piece = lax.all_gather(tokens, 'tp', axis=1, tiled=True)  7.85 us
    all_gather x1, blocking collectives, body(): gain_piece = lax.all_gather(norm_gain, 'tp', axis=1, tiled=True)  6.32 us
  transfers between devices with their start and end apart: 3, of which 2 were waited for; matrix products, arithmetic and copies ran while one was open for 7% of the time, Pallas kernels for 0%

commit v1 on v0

--- a/solution.py
+++ b/solution.py
@@ -150,7 +150,7 @@
         outgate_w,
         gate_w.reshape(model, -1),
     )
-    piece = lax.all_gather(tokens, "tp", axis=1, tiled=True)
+    piece = jnp.concatenate(lax.all_gather(tokens, "tp"), axis=1)
     gain_piece = lax.all_gather(norm_gain, "tp", axis=1, tiled=True)
     wide = piece.astype(jnp.float32)
     scaled = (wide * gain_piece.astype(jnp.float32)).astype(jnp.bfloat16)

time: 150 us -> 157 us (1.047)
  other arithmetic: 10.4 us -> 14.2 us
  local copies, waits for them, and re-layouts: 2.92 us -> 6.67 us
    convert_element_type x0 -> x2, local copies, waits for them, and re-layouts: none -> 3.9 us  [the longest x1 2.59 us: body(): wide = piece.astype(jnp.float32)]
    convert_element_type x0 -> x5, other arithmetic: none -> 3.77 us  [the longest x4 2.64 us: body(): scaled = (wide * gain_piece.astype(jnp.float32)).astype(jnp.bfloat16)]
where the time goes in v1:
time: 157 us
  blocking collectives  66.7 us (42%)
  waiting for transfers between devices  33.4 us (21%)
  matrix products  17.4 us (11%)
  between operations  14.3 us (9%)
  other arithmetic  14.2 us (9%)
  local copies, waits for them, and re-layouts  6.67 us (4%)
  starting transfers between devices  3.58 us (2%)
    all_gather x1, blocking collectives, prefix(): pieces = jax.tree.map(lambda part: lax.all_gather(part, axis), value)  27 us
    reduce_scatter x1, waiting for transfers between devices, body(): lax.psum_scatter((jnp.dot(y_conv, conv_out_w, preferred_element_type=jnp....  20.6 us
    unnamed x1, blocking collectives  19.7 us
    all_gather x1, waiting for transfers between devices, prefix(): pieces = jax.tree.map(lambda part: lax.all_gather(part, axis), value)  12.7 us
    dot_general x8, matrix products, body(): jnp.dot(scaled, weight, preferred_element_type=jnp.float32)  9.07 us
    select_n x14, other arithmetic, prefix_step(): jnp.where(position < mine, new, old)  8.88 us
    all_gather x1, blocking collectives, body(): piece = jnp.concatenate(lax.all_gather(tokens, 'tp'), axis=1)  7.85 us
    all_gather x1, blocking collectives, body(): gain_piece = lax.all_gather(norm_gain, 'tp', axis=1, tiled=True)  6.45 us
  transfers between devices with their start and end apart: 3, of which 2 were waited for; matrix products, arithmetic and copies ran while one was open for 7% of the time, Pallas kernels for 0%

profile of v1, /device:TPU:0, one launch (start us, length us, event | category | flops | bytes accessed | tf_op | source)
XLA Modules:
  0.0 156.5 jit_solution(6566375253061000092)
XLA Ops:
  6.5 6.5 %all_gather.35 = bf16[1,2048]{1,0:T(2,128)(2,1)S(1)} all-gather(bf16[1,512]{1,0:T(2,128)(2,1)} %param.18), channel_id=1, replica_groups=mesh['sp'=8,'tp'=4] {'tp'}, dimensions={1}, use_global_device_ids=true | all-gather | bytes 5120 | tf_op jit(solution)/shard_map/all_gather | solution.py:154
  13.1 0.8 slice_bitcast_fusion
  13.8 0.7 reshape.150
  14.6 7.9 %all-gather = bf16[512,512]{1,0:T(8,128)(2,1)S(1)} all-gather(bf16[128,512]{1,0:T(8,128)(2,1)} %param.17), channel_id=2, replica_groups=mesh['sp'=8,'tp'=4] {'tp'}, dimensions={0}, use_global_device_ids=true | all-gather | bytes 655360 | tf_op jit(solution)/shard_map/all_gather | solution.py:153
  22.4 0.2 fusion.21
  22.6 0.9 fusion.24
  23.5 1.3 copy.40
  24.8 0.2 convolution_multiply_fusion.8
  25.0 0.1 add_bitcast_fusion
  25.1 0.3 reduce_window_sum.14
  25.4 0.2 fusion.43
  25.6 0.2 multiply_reduce_fusion.1
  25.8 0.1 subtract_exponential_fusion.4
  25.9 1.1 convert_bitcast_fusion
  27.0 2.6 %copy.39 = f32[128,4,512]{0,2,1:T(8,128)} copy(f32[128,4,512]{2,0,1:T(8,128)} %convert_bitcast_fusion) | data formatting | bytes 2097152 | tf_op jit(solution)/shard_map/convert_element_type | solution.py:155
  29.6 1.7 %fusion.23 = bf16[128,2048]{0,1:T(8,128)(2,1)S(1)} fusion(f32[128,4,512]{0,2,1:T(8,128)} %copy.39, f32[2048]{0:T(1024)S(1)} %bitcast.242), kind=kLoop, calls=%fused_computation.49 | loop fusion | flops 524288 | bytes 1581056 | tf_op jit(solution)/shard_map/convert_element_type | solution.py:156
  31.3 2.1 %fusion.16 = bf16[128,512]{1,0:T(8,128)(2,1)S(1)} fusion(bf16[128,2048]{0,1:T(8,128)(2,1)S(1)} %fusion.23, bf16[2048,512]{1,0:T(8,128)(2,1)} %param.25, f32[128]{0:T(128)S(1)} %add_rsqrt_fusion.1), kind=kOutput, calls=%fused_computation.36 | convolution fusion | flops 268566528 | bytes 2753024 | tf_op jit(solution)/shard_map/dot_general | solution.py:159
  33.4 0.5 fusion.15
  33.9 1.3 convolution_add_fusion.1
  35.2 0.0 all-gather.8.cloned.1.call-update
  35.3 0.0 reduce-scatter.2.cloned.1.call-start
  35.3 1.6 %fusion.20 = bf16[128,256]{1,0:T(8,128)(2,1)S(1)} fusion(bf16[128,2048]{0,1:T(8,128)(2,1)S(1)} %fusion.23, bf16[2048,256]{1,0:T(8,128)(2,1)} %param.21, f32[128]{0:T(128)S(1)} %add_rsqrt_fusion.1), kind=kOutput, calls=%fused_computation.44 | convolution fusion | flops 134283264 | bytes 1638912 | tf_op jit(solution)/shard_map/dot_general | solution.py:159
  36.9 1.6 %fusion.19 = bf16[128,256]{1,0:T(8,128)(2,1)S(1)} fusion(bf16[128,2048]{0,1:T(8,128)(2,1)S(1)} %fusion.23, bf16[2048,256]{1,0:T(8,128)(2,1)} %param.20, f32[128]{0:T(128)S(1)} %add_rsqrt_fusion.1), kind=kOutput, calls=%fused_computation.43 | convolution fusion | flops 134283264 | bytes 1638912 | tf_op jit(solution)/shard_map/dot_general | solution.py:159
  38.6 3.5 %collective-permute-start = (bf16[2,256]{1,0:T(2,128)(2,1)S(1)}, bf16[2,256]{1,0:T(2,128)(2,1)S(1)}, u32[]{:S(2)}, u32[]{:S(2)}) collective-permute-start(bf16[2,256]{1,0:T(2,128)(2,1)S(1)} %slice.57), channel_id=1, source_target_pairs={{0,4},{4,8},{8,12},{12,16},{16,20},{20,24},{24,28},{1,5},{5,9},{9,... | collective-permute-start | bytes 3080 | tf_op jit(solution)/shard_map/ppermute | solution.py:17
  42.1 0.6 dynamic-slice.10
  43.4 0.2 dynamic-update-slice
  43.6 0.2 dynamic-update-slice.1
  43.8 2.3 %fusion.17 = bf16[128,512]{1,0:T(8,128)(2,1)S(1)} fusion(bf16[128,2048]{0,1:T(8,128)(2,1)S(1)} %fusion.23, bf16[2048,512]{1,0:T(8,128)(2,1)} %param.23, f32[128]{0:T(128)S(1)} %add_rsqrt_fusion.1), kind=kOutput, calls=%fused_computation.37 | convolution fusion | flops 268566528 | bytes 2753024 | tf_op jit(solution)/shard_map/dot_general | solution.py:159
  46.2 0.2 fusion.25
  46.4 0.1 fusion.57
  46.5 0.2 fusion.35
  46.7 0.3 fusion.74
  47.0 0.3 convolution_bitcast_fusion.2
  47.4 0.4 fusion.18
  47.7 0.5 fusion.14
  48.2 27.0 %all-gather.5 = f32[8,2,256]{2,1,0:T(2,128)S(1)} all-gather(f32[1,2,256]{2,1,0:T(2,128)S(1)} %fusion.57), channel_id=6, replica_groups=mesh['sp'=8,'tp'=4] {'sp'}, dimensions={0}, use_global_device_ids=true | all-gather | bytes 18432 | tf_op jit(solution)/shard_map/all_gather | solution.py:22
  75.2 19.7 %all-reduce.2 = (f32[16]{0:T(128)S(1)}, f32[16]{0:T(128)S(1)}) all-reduce(f32[16]{0:T(128)S(1)} %dynamic-update-slice, f32[16]{0:T(128)S(1)} %dynamic-update-slice.1), channel_id=3, replica_groups=mesh['sp'=8,'tp'=4] {'sp'}, use_global_device_ids=true, to_apply=%add | all-reduce | flops 32 | bytes 256
  95.0 0.1 reshape.156
  95.1 0.1 reshape.157
  95.2 2.5 %fusion.52 = f32[128,2048]{1,0:T(8,128)} fusion(bf16[256,2048]{1,0:T(8,128)(2,1)} %param.30, f32[130,256]{1,0:T(8,128)S(1)} %maximum_convert_fusion, bf16[128,256]{1,0:T(8,128)(2,1)S(1)} %fusion.18, f32[256]{0:T(256)S(1)} %bitcast.246, f32[256]{0:T(256)S(1)} %bitcast.245, f32[256]{0:T(256)S(1)} %bitcast.244), kind=kOutput, calls=%fused_computation.89 | convolution fusion | flops 134479872 | bytes 2558976 | tf_op jit(solution)/shard_map/dot_general | solution.py:208
  97.7 12.7 %all-gather.8.cloned.1.call-done = f32[16,256,256]{2,1,0:T(8,128)} async-done(((f32[2,256,256]{2,1,0:T(8,128)}), f32[16,256,256]{2,1,0:T(8,128)}) %all-gather.8.cloned.1.call-update) | async-done | bytes 4194320 | tf_op jit(solution)/shard_map/all_gather | solution.py:22
  110.5 9.3 %while.5 = (s32[]{:T(128)}, f32[2]{0:T(128)S(1)}, f32[2,256,256]{2,1,0:T(8,128)S(1)}, f32[2,256]{1,0:T(2,128)S(1)}, s32[]{:T(128)}, /*index=5*/f32[8,2]{1,0:T(8,...) while((s32[]{:T(128)}, f32[2]{0:T(128)S(1)}, ...), condition=%wide.region_4.5_spmd.clone, body=%wide.region_3.4_spmd.clone.sunk | while | flops 657940 | bytes 1579278 | solution.py:31
  110.5 0.1 fusion.99
  110.6 1.2 fusion.98
  111.8 0.1 fusion.99
  111.9 1.2 fusion.98
  113.2 0.1 fusion.99
  113.3 1.2 fusion.98
  114.5 0.1 fusion.99
  114.6 1.2 fusion.98
  115.8 0.1 fusion.99
  115.9 1.2 fusion.98
  117.2 0.1 fusion.99
  117.3 1.2 fusion.98
  118.5 0.1 fusion.99
  118.6 1.2 fusion.98
  119.8 0.2 fusion.33
  120.0 0.1 fusion.65
  120.1 0.3 fusion.13
  120.4 0.5 multiply_reduce_fusion
  120.8 5.7 %psum.7 = f32[128]{0:T(128)S(1)} all-reduce(f32[128]{0:T(128)S(1)} %get-tuple-element.276), channel_id=1, replica_groups=mesh['sp'=8,'tp'=4] {'tp'}, use_global_device_ids=true, to_apply=%region_7.8 | all-reduce | flops 128 | bytes 1024 | tf_op jit(solution)/shard_map/psum | solution.py:202
  126.5 2.5 %fusion.7 = bf16[128,2048]{1,0:T(8,128)(2,1)} fusion(f32[128,2048]{1,0:T(8,128)} %fusion.52, bf16[512,2048]{1,0:T(8,128)(2,1)S(1)} %copy-done, f32[128,512]{1,0:T(8,128)S(1)} %bitcast.234, bf16[128,512]{1,0:T(8,128)(2,1)S(1)} %fusion.14, f32[512]{0:T(512)S(1)} %convert_element_type.112, f32[128]{0:T(128)S(1)} %add_rsqrt_fusion), kind=kOutput, calls=%fused_computation.16 | convolution fusion | flops 269484032 | bytes 4065792 | tf_op jit(solution)/shard_map/dot_general | solution.py:209
  129.1 0.0 reduce-scatter.2.cloned.1.call-update
  129.1 20.6 %reduce-scatter.2.cloned.1.call-done = bf16[32,2048]{1,0:T(8,128)(2,1)} async-done(((bf16[128,2048]{1,0:T(8,128)(2,1)}), bf16[32,2048]{1,0:T(8,128)(2,1)}) %reduce-scatter.2.cloned.1.call-update) | async-done | bytes 131088 | tf_op jit(solution)/shard_map/reduce_scatter | solution.py:206
  (50 shorter events, 0.5 us)
Async XLA Ops:
  6.5 120.0 %copy-start = (bf16[512,2048]{1,0:T(8,128)(2,1)S(1)}, bf16[512,2048]{1,0:T(8,128)(2,1)}, u32[]{:S(2)}) copy-start(bf16[512,2048]{1,0:T(8,128)(2,1)} %param.31) | copy-start | bytes 6291460
  6.5 103.9 %all-gather.8.cloned.1.call-start = ((), (), s32[]{:S(2)}) async-start(), calls=%async_computation.2 | async-start | bytes 4718592 | tf_op jit(solution)/shard_map/all_gather | solution.py:22
  29.6 3.8 %copy-start.1 = (bf16[2048,512]{1,0:T(8,128)(2,1)S(1)}, bf16[2048,512]{1,0:T(8,128)(2,1)}, u32[]{:S(2)}) copy-start(bf16[2048,512]{1,0:T(8,128)(2,1)} %param.24) | copy-start | bytes 6291460
  35.2 6.9 %copy-start.6 = (u32[32]{0:T(128)S(1)}, u32[32]{0:T(128)}, u32[]{:S(2)}) copy-start(u32[32]{0:T(128)} %constant.86) | copy-start | bytes 388
  35.3 114.4 %reduce-scatter.2.cloned.1.call-start = ((), (), s32[]{:S(2)}) async-start(), calls=%async_computation.1 | async-start | bytes 655360 | tf_op jit(solution)/shard_map/reduce_scatter | solution.py:206
  36.9 9.6 %copy-start.4 = (bf16[3,256]{1,0:T(4,128)(2,1)S(1)}, bf16[3,256]{1,0:T(4,128)(2,1)}, u32[]{:S(2)}) copy-start(bf16[3,256]{1,0:T(4,128)(2,1)} %param.22) | copy-start | bytes 4612
  38.6 56.6 %collective-permute-start = (bf16[2,256]{1,0:T(2,128)(2,1)S(1)}, bf16[2,256]{1,0:T(2,128)(2,1)S(1)}, u32[]{:S(2)}, u32[]{:S(2)}) collective-permute-start(bf16[2,256]{1,0:T(2,128)(2,1)S(1)} %slice.57), channel_id=1, source_target_pairs={{0,4},{4,8},{8,12},{12,16},{16,20},{20,24},{24,28},{1,5},{5,9},{9,... | collective-permute-start | bytes 3080 | tf_op jit(solution)/shard_map/ppermute | solution.py:17
  43.8 3.5 %copy-start.3 = (bf16[2048,256]{1,0:T(8,128)(2,1)S(1)}, bf16[2048,256]{1,0:T(8,128)(2,1)}, u32[]{:S(2)}) copy-start(bf16[2048,256]{1,0:T(8,128)(2,1)} %param.19) | copy-start | bytes 3145732
  46.1 1.6 %copy-start.2 = (bf16[2048,512]{1,0:T(8,128)(2,1)S(1)}, bf16[2048,512]{1,0:T(8,128)(2,1)}, u32[]{:S(2)}) copy-start(bf16[2048,512]{1,0:T(8,128)(2,1)} %param.26) | copy-start | bytes 6291460
  47.3 47.6 %copy-start.5 = (bf16[512]{0:T(512)(128)(2,1)S(1)}, bf16[512]{0:T(512)(128)(2,1)}, u32[]{:S(2)}) copy-start(bf16[512]{0:T(512)(128)(2,1)} %param.29) | copy-start | bytes 3076
Sparse Core Ops, SparseCore 0:
  35.4 75.0 all-gather.7
  129.2 20.4 reduce-scatter.1
